TPU v7x, 32 devices: a whole 2x2x4 slice. The times are simulated.
32 devices in a mesh: sp: 16 (over z, y, x), tp: 2 (over core).
Axes of the slice: x: 2, y: 2, z: 4, core: 2. Of those that a mesh axis runs over, the one named last changes fastest.
Arguments:
- residual: bfloat16 [4096, 2048], P(('sp', 'tp')), may hold values from -6 to 6
- query_nope: bfloat16 [4096, 1024], P('sp', 'tp'), may hold values from -24 to 24
- query_rope: bfloat16 [4096, 512], P('sp', 'tp'), may hold values from -400 to 400
- latent: bfloat16 [4096, 256], P(('sp', 'tp')), may hold values from -6 to 6
- key_rope: bfloat16 [4096, 64], P(('sp', 'tp')), may hold values from -6 to 6
- key_up: bfloat16 [256, 1024], P(None, 'tp'), may hold values from -0.375 to 0.375
- value_up: bfloat16 [256, 1024], P(None, 'tp'), may hold values from -0.375 to 0.375
- out_proj: bfloat16 [1024, 2048], replicated, may hold values from -0.375 to 0.375
- norm_gain: float32 [2048], replicated, may hold values from 0.1 to 1.9
- routes: int32 [4096, 2], P(('sp', 'tp')), may hold values from 0 to 15, all different within a row; in each aligned block of 128 rows (0 to 127, 128 to 255, ...) at most 32 rows name the same one
- route_weight: float32 [4096, 2], P(('sp', 'tp')), may hold values from 0.3 to 2.5
- w_gate: bfloat16 [16, 2048, 512], P('sp', None, 'tp'), may hold values from -0.125 to 0.125
- w_up: bfloat16 [16, 2048, 512], P('sp', None, 'tp'), may hold values from -0.125 to 0.125
- w_down: bfloat16 [16, 512, 2048], P('sp', 'tp'), may hold values from -0.25 to 0.25
Outputs:
- mixed: bfloat16 [4096, 2048], P(('sp', 'tp'))
Inputs may be any that keep to these rules, and one draw needn't show every extreme that they name: `routes`: each row names 2 different experts. Among the rows of one device no expert is named more than 32 times, a bound that some block reaches by the rows of some device.
All inputs are finite; a program needn't handle non-finite values.
Results may differ from a plain program's by a relative error of at most 0.015.
Values may be sent and summed in bfloat16 or wider, within the bound.
A program may use at most 128 MiB of HBM per device.

v0:
```python
import jax
import jax.numpy as jnp
from jax import lax
from jax.sharding import PartitionSpec as P

QK_NOPE = 128
QK_ROPE = 64
V_DIM = 128
SEGMENT = 64
EPSILON = 1e-06
ROPE_BASE = 10000.0
NEG_LARGE = -1e30


def rotary(values, positions):
    half_width = values.shape[-1] // 2
    inverse = ROPE_BASE ** (-2.0 * jnp.arange(half_width, dtype=jnp.float32) / values.shape[-1])
    angles = positions.astype(jnp.float32)[:, None] * inverse[None, :]
    cosine = jnp.cos(angles)
    sine_part = jnp.sin(angles)
    if values.ndim == 3:
        cosine = cosine[:, None, :]
        sine_part = sine_part[:, None, :]
    first_half = values[..., :half_width]
    second = values[..., half_width:]
    return jnp.concatenate(
        [first_half * cosine - second * sine_part, second * cosine + first_half * sine_part],
        axis=-1,
    )


def local(
    residual,
    query_nope,
    query_rope,
    latent,
    key_rope,
    key_up,
    value_up,
    out_proj,
    norm_gain,
    routes,
    route_weight,
    w_gate,
    w_up,
    w_down,
):
    tp_count = lax.axis_size("tp")
    tp_index = lax.axis_index("tp")
    sp_index = lax.axis_index("sp")
    row_count = residual.shape[0]
    tok_dev = query_nope.shape[0]
    heads_here = query_nope.shape[1] // QK_NOPE
    score_scale = (QK_NOPE + QK_ROPE) ** (-0.5)
    query_first = sp_index * tok_dev
    query_pos = query_first + jnp.arange(tok_dev, dtype=jnp.int32)
    query_rot = rotary(
        query_rope.astype(jnp.float32).reshape(tok_dev, heads_here, QK_ROPE), query_pos
    ).astype(jnp.bfloat16)
    query_heads = query_nope.reshape(tok_dev, heads_here, QK_NOPE)
    key_pos = query_first + tp_index * row_count + jnp.arange(row_count, dtype=jnp.int32)
    key_rot = rotary(key_rope.astype(jnp.float32), key_pos).astype(jnp.bfloat16)
    query_segment = query_pos // SEGMENT
    last_segment = (query_first + tok_dev - 1) // SEGMENT
    initial = (
        jnp.full((heads_here, tok_dev), NEG_LARGE, jnp.float32),
        jnp.zeros((heads_here, tok_dev), jnp.float32),
        jnp.zeros((tok_dev, heads_here, V_DIM), jnp.float32),
    )
    paired = (
        lax.all_gather(latent, "tp", axis=0, tiled=True),
        lax.all_gather(key_rot, "tp", axis=0, tiled=True),
    )
    lat_rows = lax.all_gather(paired[0], "sp", axis=0, tiled=True)
    rot_rows = lax.all_gather(paired[1], "sp", axis=0, tiled=True)
    piece_rows = lat_rows.shape[0]
    key_block = piece_rows
    while key_block > 2048 and key_block % 2 == 0:
        key_block //= 2
    block_count = piece_rows // key_block

    def one_block(state_now, inputs):
        lat_block, rot_block, offset = inputs
        key_nope = jnp.dot(lat_block, key_up, preferred_element_type=jnp.float32).astype(
            jnp.bfloat16
        )
        key_nope = key_nope.reshape(key_block, heads_here, QK_NOPE)
        value_rows = jnp.dot(lat_block, value_up, preferred_element_type=jnp.float32).astype(
            jnp.bfloat16
        )
        value_rows = value_rows.reshape(key_block, heads_here, V_DIM)
        scores = jnp.einsum(
            "qhd,khd->hqk", query_heads, key_nope, preferred_element_type=jnp.float32
        )
        scores = (
            scores
            + jnp.einsum("qhr,kr->hqk", query_rot, rot_block, preferred_element_type=jnp.float32)
        ) * score_scale
        key_segment = (offset + jnp.arange(key_block, dtype=jnp.int32)) // SEGMENT
        allowed = (key_segment[None, :] <= query_segment[:, None])[None]
        scores = jnp.where(allowed, scores, NEG_LARGE)
        old_max, old_sum, old_acc = state_now
        new_max = jnp.maximum(old_max, jnp.max(scores, axis=-1))
        weights = jnp.where(allowed, jnp.exp(scores - new_max[:, :, None]), 0.0)
        shrink = jnp.exp(old_max - new_max)
        new_sum = old_sum * shrink + jnp.sum(weights, axis=-1)
        new_acc = old_acc * shrink.T[:, :, None] + jnp.einsum(
            "hqk,khv->qhv",
            weights.astype(jnp.bfloat16),
            value_rows,
            preferred_element_type=jnp.float32,
        )
        return ((new_max, new_sum, new_acc), None)

    def compute(state_now):
        result, unused = lax.scan(
            one_block,
            state_now,
            (
                lat_rows.reshape(block_count, key_block, lat_rows.shape[1]),
                rot_rows.reshape(block_count, key_block, rot_rows.shape[1]),
                jnp.arange(block_count, dtype=jnp.int32) * key_block,
            ),
        )
        return result

    def keep_state(state_now):
        return state_now

    row_max, weight_sum, weighted = lax.cond(
        jnp.int32(0) // SEGMENT <= last_segment, compute, keep_state, initial
    )
    attn_out = (
        (weighted / weight_sum.T[:, :, None])
        .astype(jnp.bfloat16)
        .reshape(tok_dev, heads_here * V_DIM)
    )
    all_heads = lax.all_to_all(attn_out, "tp", split_axis=0, concat_axis=1, tiled=True)
    projected = jnp.dot(all_heads, out_proj, preferred_element_type=jnp.float32)
    hidden_wide = residual.astype(jnp.float32) + projected
    hidden = hidden_wide.astype(jnp.bfloat16)
    hidden_wide = hidden.astype(jnp.float32)
    normed = hidden_wide * lax.rsqrt(
        jnp.mean(hidden_wide * hidden_wide, axis=-1, keepdims=True) + EPSILON
    )
    normed = (normed * norm_gain[None, :]).astype(jnp.bfloat16)
    expert_count = lax.axis_size("sp")
    capacity = max(2, 2 * (row_count * tp_count) // expert_count)
    top_count = routes.shape[1]
    width = normed.shape[1]
    flat_expert = routes.reshape(-1)
    onehot = (flat_expert[:, None] == jnp.arange(expert_count, dtype=jnp.int32)[None, :]).astype(
        jnp.int32
    )
    slot_rank = jnp.sum(jnp.cumsum(onehot, axis=0) * onehot, axis=1) - 1
    slot_index = flat_expert * capacity + slot_rank
    outgoing = (
        jnp.zeros((expert_count * capacity, width), jnp.bfloat16)
        .at[slot_index]
        .set(jnp.repeat(normed, top_count, axis=0))
    )
    gate_weight = w_gate[0]
    up_weight = w_up[0]
    down_weight = w_down[0]
    shard_piece = lax.all_gather(
        lax.all_to_all(
            outgoing.reshape(expert_count, capacity, width),
            "sp",
            split_axis=0,
            concat_axis=0,
            tiled=True,
        ),
        "tp",
        axis=0,
        tiled=True,
    )
    gate_part = jnp.dot(shard_piece, gate_weight, preferred_element_type=jnp.float32)
    up_part = jnp.dot(shard_piece, up_weight, preferred_element_type=jnp.float32)
    activated = (jax.nn.silu(gate_part) * up_part).astype(jnp.bfloat16)
    product = jnp.dot(activated, down_weight, preferred_element_type=jnp.float32)
    summed = lax.psum_scatter(
        lax.optimization_barrier(product.astype(jnp.bfloat16))
        .astype(jnp.float32)
        .astype(jnp.bfloat16),
        "tp",
        scatter_dimension=0,
        tiled=True,
    )
    back_rows = lax.all_to_all(summed, "sp", split_axis=0, concat_axis=0, tiled=True)
    picked = back_rows.reshape(expert_count * capacity, width)[slot_index]
    combined = jnp.sum(
        picked.astype(jnp.float32).reshape(row_count, top_count, width) * route_weight[:, :, None],
        axis=1,
    )
    return (hidden_wide + combined).astype(jnp.bfloat16)


def solution(mesh):
    return jax.shard_map(
        local,
        mesh=mesh,
        in_specs=(
            P(("sp", "tp"), None),
            P("sp", "tp"),
            P("sp", "tp"),
            P(("sp", "tp"), None),
            P(("sp", "tp"), None),
            P(None, "tp"),
            P(None, "tp"),
            P(),
            P(),
            P(("sp", "tp"), None),
            P(("sp", "tp"), None),
            P("sp", None, "tp"),
            P("sp", None, "tp"),
            P("sp", "tp", None),
        ),
        out_specs=P(("sp", "tp"), None),
        check_vma=False,
    )
```

profile of v0, /device:TPU:12, one launch (start us, length us, event | category | flops | bytes accessed | tf_op | source)
XLA Modules:
  0.0 297.6 jit_solution(12448938111200499188)
XLA Ops:
  6.5 3.5 %all_gather.15 = bf16[256,256]{1,0:T(8,128)(2,1)} all-gather(bf16[128,256]{1,0:T(8,128)(2,1)} %param.21), channel_id=1, replica_groups=mesh['sp'=16,'tp'=2] {'tp'}, dimensions={0}, use_global_device_ids=true | all-gather | bytes 196608 | tf_op jit(solution)/shard_map/all_gather | solution.py:71
  10.1 0.8 copy.59
  11.2 1.0 copy.54
  12.2 0.7 convert_element_type.81
  12.9 0.6 reduce-window.6
  13.7 0.7 broadcast_multiply_fusion
  14.9 1.9 all_gather.17
  17.1 35.9 %all_gather.18 = bf16[4096,64]{0,1:T(8,128)(2,1)S(1)} all-gather(bf16[256,64]{0,1:T(8,128)(2,1)S(1)} %all_gather.17), channel_id=1, replica_groups=mesh['sp'=16,'tp'=2] {'sp'}, dimensions={0}, use_global_device_ids=true | all-gather | bytes 557056 | tf_op jit(solution)/shard_map/all_gather | solution.py:75
  53.0 20.2 %all-gather.3.cloned.1.call-done = bf16[4096,256]{1,0:T(8,128)(2,1)} async-done(((bf16[256,256]{1,0:T(8,128)(2,1)}), bf16[4096,256]{1,0:T(8,128)(2,1)}) %all-gather.3.cloned.1.call-update) | async-done | bytes 2097168 | tf_op jit(solution)/shard_map/all_gather | solution.py:74
  73.2 44.0 %conditional.1 = (f32[4,256]{1,0:T(4,128)}, f32[256,4,128]{0,2,1:T(8,128)}) conditional(s32[]{:T(128)} %convert_element_type.80, () %tuple.28, (bf16[4096,256]{1,0:T(8,128)(2,1)}, bf16[4096,64]{0,1:T(8,128)(2,1)S(1)}, bf16[256,512]{1,0:T(8,128)(2,1)}, s32[256]{0:T(256)S(1)}, s32[256]{0:T(256)S(1)}, /*index=5*/s32[]{:T(128)}, ...), branch_computations={%region_0.1_spmd, %region_1.6_spmd.clone} | conditional | flops 2439948032 | bytes 85153152 | solution.py:130
  73.3 1.1 copy.55
  74.6 42.6 %while.20 = (s32[]{:T(128)}, f32[4,256]{1,0:T(4,128)S(1)}, f32[4,256]{1,0:T(4,128)}, f32[256,4,128]{0,2,1:T(8,128)}, s32[2]{0:T(128)S(1)}, /*index=5*/s32[256]{0...) while((s32[]{:T(128)}, f32[4,256]{1,0:T(4,128)S(1)}, ...), condition=%wide.region_5.5_spmd.clone, body=%wide.region_2.4_spmd.clone.sunk | while | flops 2439944192 | bytes 83052784 | solution.py:116
  74.6 2.0 convolution_convert_fusion.5
  76.6 1.3 fusion.95
  77.9 0.7 dynamic_slice.45
  78.6 0.6 add_select_fusion.2
  79.7 5.5 %fusion.96 = (f32[4,256]{1,0:T(4,128)S(1)}, f32[4,256,2048]{1,2,0:T(8,128)}) fusion(bf16[256,4,64]{0,2,1:T(8,128)(2,1)S(1)} %get-tuple-element.537, bf16[2,2048,64]{1,2,0:T(8,128)(2,1)S(1)} %get-tuple-element.536, s32[]{:T(128)} %get-tuple-element.513, f32[4,2048,256]{2,1,0:T(8,128)S(1)} %fusion.95, pred[256,2048]{0,1:T(8,128)(4,1)S(1)} %broadcast_compare_fusion.2), kind=kOutput, calls=%fused_computation.105.clone.1 | convolution fusion | flops 276823040 | bytes 17698820 | tf_op jit(solution)/shard_map/cond/branch_1_fun/while/body/eval_jaxpr/qhr,kr->hqk/dot_general | solution.py:97
  85.2 2.1 convolution_convert_fusion.6
  87.4 6.0 %fusion.100 = f32[256,4,128]{0,2,1:T(8,128)} fusion(bf16[2048,4,128]{0,2,1:T(8,128)(2,1)S(1)} %bitcast.115, f32[4,256,2048]{1,2,0:T(8,128)} %get-tuple-element.497, f32[4,256]{1,0:T(4,128)S(1)} %get-tuple-element.528, pred[256,2048]{0,1:T(8,128)(4,1)S(1)} %broadcast_compare_fusion.2, f32[256,4,128]{0,2,1:T(8,128)} %get-tuple-element.516, ...), kind=kOutput, calls=%fused_computation.15.clone.1 | convolution fusion | flops 543555584 | bytes 12066817 | tf_op jit(solution)/shard_map/cond/branch_1_fun/while/body/eval_jaxpr/hqk,khv->qhv/dot_general | solution.py:107
  93.4 1.5 fusion.98
  94.9 0.6 fusion.99
  95.5 2.0 convolution_convert_fusion.5
  97.6 1.3 fusion.95
  98.9 0.7 dynamic_slice.45
  99.5 0.6 add_select_fusion.2
  100.6 5.5 %fusion.96 = (f32[4,256]{1,0:T(4,128)S(1)}, f32[4,256,2048]{1,2,0:T(8,128)}) fusion(bf16[256,4,64]{0,2,1:T(8,128)(2,1)S(1)} %get-tuple-element.537, bf16[2,2048,64]{1,2,0:T(8,128)(2,1)S(1)} %get-tuple-element.536, s32[]{:T(128)} %get-tuple-element.513, f32[4,2048,256]{2,1,0:T(8,128)S(1)} %fusion.95, pred[256,2048]{0,1:T(8,128)(4,1)S(1)} %broadcast_compare_fusion.2), kind=kOutput, calls=%fused_computation.105.clone.1 | convolution fusion | flops 276823040 | bytes 17698820 | tf_op jit(solution)/shard_map/cond/branch_1_fun/while/body/eval_jaxpr/qhr,kr->hqk/dot_general | solution.py:97
  106.2 2.1 convolution_convert_fusion.6
  108.3 6.1 %fusion.100 = f32[256,4,128]{0,2,1:T(8,128)} fusion(bf16[2048,4,128]{0,2,1:T(8,128)(2,1)S(1)} %bitcast.115, f32[4,256,2048]{1,2,0:T(8,128)} %get-tuple-element.497, f32[4,256]{1,0:T(4,128)S(1)} %get-tuple-element.528, pred[256,2048]{0,1:T(8,128)(4,1)S(1)} %broadcast_compare_fusion.2, f32[256,4,128]{0,2,1:T(8,128)} %get-tuple-element.516, ...), kind=kOutput, calls=%fused_computation.15.clone.1 | convolution fusion | flops 543555584 | bytes 12066817 | tf_op jit(solution)/shard_map/cond/branch_1_fun/while/body/eval_jaxpr/hqk,khv->qhv/dot_general | solution.py:107
  114.4 1.5 fusion.98
  115.9 1.3 fusion.99
  117.2 1.1 divide_convert_fusion
  118.5 3.9 %all_to_all.29 = bf16[2,128,512]{2,1,0:T(8,128)(2,1)S(1)} all-to-all(bf16[2,128,512]{2,1,0:T(8,128)(2,1)S(1)} %copy.65), channel_id=1, replica_groups=mesh['sp'=16,'tp'=2] {'tp'}, dimensions={0} | all-to-all | bytes 524288 | tf_op jit(solution)/shard_map/all_to_all | solution.py:138
  122.7 3.1 %multiply_reduce_fusion.1 = (f32[128]{0:T(128)S(1)}, f32[128,2048]{1,0:T(8,128)S(1)}) fusion(bf16[128,1024]{0,1:T(8,128)(2,1)S(1)} %bitcast.120, bf16[1024,2048]{1,0:T(8,128)(2,1)} %param.25, bf16[128,2048]{1,0:T(8,128)(2,1)} %param.18), kind=kOutput, calls=%fused_computation.66 | convolution fusion | flops 538443648 | bytes 6029824 | tf_op jit(solution)/shard_map/dot_general | solution.py:139
  125.8 1.0 copy-done.1
  127.0 0.6 broadcast_in_dim.71
  127.6 1.2 reshape.245
  128.9 3.5 %scatter_custom_fusion = bf16[512,2048]{1,0:T(8,128)(2,1)S(1)} fusion(s32[256]{0:T(256)S(1)} %bitcast.123, bf16[256,2048]{1,0:T(8,128)(2,1)} %reshape.245, bf16[]{:T(256)} %constant.158.clone.1), kind=kCustom, calls=%fused_computation.67 | custom fusion | bytes 2097664 | tf_op jit(solution)/shard_map/scatter | solution.py:160
  132.4 52.8 %all_to_all.30 = bf16[16,32,2048]{2,1,0:T(8,128)(2,1)} all-to-all(bf16[16,32,2048]{2,1,0:T(8,128)(2,1)S(1)} %bitcast.116), channel_id=1, replica_groups=mesh['sp'=16,'tp'=2] {'sp'}, dimensions={0} | all-to-all | bytes 4194304 | tf_op jit(solution)/shard_map/all_to_all | solution.py:166
  185.2 13.1 %all-gather.5.cloned.1.call-done = bf16[32,32,2048]{2,1,0:T(8,128)(2,1)} async-done(((bf16[16,32,2048]{2,1,0:T(8,128)(2,1)}), bf16[32,32,2048]{2,1,0:T(8,128)(2,1)}) %all-gather.5.cloned.1.call-update) | async-done | bytes 4194320 | tf_op jit(solution)/shard_map/all_gather | solution.py:165
  198.3 3.7 %fusion.36 = f32[32,32,256]{2,1,0:T(8,128)S(1)} fusion(bf16[32,32,2048]{2,1,0:T(8,128)(2,1)} %all-gather.5.cloned.1.call-done, bf16[1,2048,256]{2,1,0:T(8,128)(2,1)} %param.29), kind=kOutput, calls=%fused_computation.57 | convolution fusion | flops 1073741824 | bytes 6291456 | tf_op jit(solution)/shard_map/dot_general | solution.py:177
  202.1 8.5 %convolution_convert_fusion.2 = bf16[32,32,2048]{2,1,0:T(8,128)(2,1)} fusion(bf16[32,32,2048]{2,1,0:T(8,128)(2,1)} %all-gather.5.cloned.1.call-done, bf16[1,256,2048]{2,1,0:T(8,128)(2,1)S(1)} %copy-done, bf16[1,2048,256]{2,1,0:T(8,128)(2,1)S(1)} %copy-done.6, f32[32,32,256]{2,1,0:T(8,128)S(1)} %fusion.36), kind=kOutput, calls=%fused_computation.48 | convolution fusion | flops 2151153664 | bytes 11534336 | tf_op jit(solution)/shard_map/dot_general | solution.py:180
  210.6 13.5 %reduce-scatter.2.cloned.1.call-done = bf16[16,32,2048]{2,1,0:T(8,128)(2,1)} async-done(((bf16[32,32,2048]{2,1,0:T(8,128)(2,1)}), bf16[16,32,2048]{2,1,0:T(8,128)(2,1)}) %reduce-scatter.2.cloned.1.call-update) | async-done | bytes 2097168 | tf_op jit(solution)/shard_map/reduce_scatter | solution.py:181
  224.1 7.0 %all-to-all-start.2 = ((bf16[16,32,2048]{2,1,0:T(8,128)(2,1)}), bf16[16,32,2048]{2,1,0:T(8,128)(2,1)S(1)}, u32[]{:S(2)}, u32[]{:S(2)}) async-start(bf16[16,32,2048]{2,1,0:T(8,128)(2,1)} %reduce-scatter.2.cloned.1.call-done), calls=%async_computation.3 | async-start | bytes 4194304 | tf_op jit(solution)/shard_map/all_to_all | solution.py:189
  231.2 48.3 %all-to-all-done.2 = bf16[16,32,2048]{2,1,0:T(8,128)(2,1)S(1)} async-done(((bf16[16,32,2048]{2,1,0:T(8,128)(2,1)}), bf16[16,32,2048]{2,1,0:T(8,128)(2,1)S(1)}, u32[]{:S(2)}, u32[]{:S(2)}) %all-to-all-start.2) | async-done | bytes 2097184 | tf_op jit(solution)/shard_map/all_to_all | solution.py:189
  279.4 2.4 gather_fusion
  281.8 3.5 %reshape.232 = f32[128,2,2048]{2,1,0:T(2,128)} reshape(bf16[256,2048]{1,0:T(8,128)(2,1)} %gather_fusion) | data formatting | bytes 3145728 | tf_op jit(solution)/shard_map/convert_element_type | solution.py:192
  285.3 4.8 %multiply_reduce_fusion = f32[128,2048]{1,0:T(8,128)S(1)} fusion(f32[128,2,2048]{2,1,0:T(2,128)} %reshape.232, f32[128,2]{1,0:T(8,128)S(1)} %copy.62), kind=kLoop, calls=%fused_computation.52 | loop fusion | flops 786432 | bytes 3146752 | tf_op jit(solution)/shard_map/reduce_sum | solution.py:191
  290.1 0.9 add_convert_fusion
  (71 shorter events, 3.3 us)
Async XLA Ops:
  6.5 195.5 %copy-start = (bf16[1,256,2048]{2,1,0:T(8,128)(2,1)S(1)}, bf16[1,256,2048]{2,1,0:T(8,128)(2,1)}, u32[]{:S(2)}) copy-start(bf16[1,256,2048]{2,1,0:T(8,128)(2,1)} %param.31) | copy-start | bytes 3145732
  6.5 66.7 %all-gather.3.cloned.1.call-start = ((), (), s32[]{:S(2)}) async-start(), calls=%async_computation.4 | async-start | bytes 2228224 | tf_op jit(solution)/shard_map/all_gather | solution.py:74
  10.0 188.3 %all-gather.5.cloned.1.call-start = ((), (), s32[]{:S(2)}) async-start(), calls=%async_computation.5 | async-start | bytes 6291456 | tf_op jit(solution)/shard_map/all_gather | solution.py:165
  79.7 5.5 %copy-start.3 = (bf16[256,512]{1,0:T(8,128)(2,1)S(1)}, bf16[256,512]{1,0:T(8,128)(2,1)}, u32[]{:S(2)}) copy-start(bf16[256,512]{1,0:T(8,128)(2,1)} %get-tuple-element.538) | copy-start | bytes 786436 | tf_op jit(solution)/shard_map/cond/branch_1_fun/while
  85.2 8.2 %slice-start = ((s8[8388608]{0:T(1024)(128)(4,1)}), s8[4194304]{0:T(1024)(128)(4,1)S(1)}, s32[]{:S(2)}) async-start(s8[8388608]{0:T(1024)(128)(4,1)} %bitcast.110), calls=%async_computation.7 | async-start | bytes 8388608 | tf_op jit(solution)/shard_map/cond/branch_1_fun/while
  87.4 6.0 %slice-start.1 = ((s8[8388608]{0:T(1024)(128)(4,1)}), s8[4194304]{0:T(1024)(128)(4,1)S(1)}, s32[]{:S(2)}) async-start(s8[8388608]{0:T(1024)(128)(4,1)} %bitcast.110), calls=%async_computation.8 | async-start | bytes 8388608 | tf_op jit(solution)/shard_map/cond/branch_1_fun/while
  100.6 5.5 %copy-start.3 = (bf16[256,512]{1,0:T(8,128)(2,1)S(1)}, bf16[256,512]{1,0:T(8,128)(2,1)}, u32[]{:S(2)}) copy-start(bf16[256,512]{1,0:T(8,128)(2,1)} %get-tuple-element.538) | copy-start | bytes 786436 | tf_op jit(solution)/shard_map/cond/branch_1_fun/while
  106.2 8.2 %slice-start = ((s8[8388608]{0:T(1024)(128)(4,1)}), s8[4194304]{0:T(1024)(128)(4,1)S(1)}, s32[]{:S(2)}) async-start(s8[8388608]{0:T(1024)(128)(4,1)} %bitcast.110), calls=%async_computation.7 | async-start | bytes 8388608 | tf_op jit(solution)/shard_map/cond/branch_1_fun/while
  108.3 6.1 %slice-start.1 = ((s8[8388608]{0:T(1024)(128)(4,1)}), s8[4194304]{0:T(1024)(128)(4,1)S(1)}, s32[]{:S(2)}) async-start(s8[8388608]{0:T(1024)(128)(4,1)} %bitcast.110), calls=%async_computation.8 | async-start | bytes 8388608 | tf_op jit(solution)/shard_map/cond/branch_1_fun/while
  118.3 8.6 %copy-start.4 = (f32[2048]{0:T(1024)S(1)}, f32[2048]{0:T(1024)}, u32[]{:S(2)}) copy-start(f32[2048]{0:T(1024)} %param.26) | copy-start | bytes 24580
  125.8 1.1 copy-start.1
  185.2 16.9 %copy-start.6 = (bf16[1,2048,256]{2,1,0:T(8,128)(2,1)S(1)}, bf16[1,2048,256]{2,1,0:T(8,128)(2,1)}, u32[]{:S(2)}) copy-start(bf16[1,2048,256]{2,1,0:T(8,128)(2,1)} %param.30) | copy-start | bytes 3145732
  185.2 38.9 %reduce-scatter.2.cloned.1.call-start = ((), (), s32[]{:S(2)}) async-start(), calls=%async_computation.6 | async-start | bytes 6291456 | tf_op jit(solution)/shard_map/reduce_scatter | solution.py:181
  210.6 20.5 %copy-start.5 = (f32[128,2]{0,1:T(2,128)S(1)}, f32[128,2]{0,1:T(2,128)}, u32[]{:S(2)}) copy-start(f32[128,2]{0,1:T(2,128)} %param.28) | copy-start | bytes 3076
  224.1 55.4 %all-to-all-start.2 = ((bf16[16,32,2048]{2,1,0:T(8,128)(2,1)}), bf16[16,32,2048]{2,1,0:T(8,128)(2,1)S(1)}, u32[]{:S(2)}, u32[]{:S(2)}) async-start(bf16[16,32,2048]{2,1,0:T(8,128)(2,1)} %reduce-scatter.2.cloned.1.call-done), calls=%async_computation.3 | async-start | bytes 4194304 | tf_op jit(solution)/shard_map/all_to_all | solution.py:189
  281.8 8.3 %copy-start.2 = (f32[128,2048]{1,0:T(8,128)S(1)}, f32[128,2048]{1,0:T(8,128)}, u32[]{:S(2)}) copy-start(f32[128,2048]{1,0:T(8,128)} %copy-done.1) | copy-start | bytes 3145732
Sparse Core Ops, SparseCore 0:
  10.2 63.0 all-gather.2
  185.3 12.9 all-gather.4
  210.7 13.2 reduce-scatter.1
where the time goes:
time: 298 us
  blocking collectives  97.9 us (33%)
  waiting for transfers between devices  95.1 us (32%)
  matrix products  49.3 us (17%)
  local copies, waits for them, and re-layouts  17.9 us (6%)
  other arithmetic  16.7 us (6%)
  between operations  13.3 us (4%)
  starting transfers between devices  7.08 us (2%)
    all_to_all x1, blocking collectives, local(): lax.all_to_all(outgoing.reshape(expert_count, capacity, width), 'sp', spl...  52.8 us
    all_to_all x1, waiting for transfers between devices, local(): lax.all_to_all(summed, 'sp', split_axis=0, concat_axis=0, tiled=True)  48.3 us
    all_gather x1, blocking collectives, local(): rot_rows = lax.all_gather(paired[1], 'sp', axis=0, tiled=True)  35.9 us
    all_gather x1, waiting for transfers between devices, local(): lat_rows = lax.all_gather(paired[0], 'sp', axis=0, tiled=True)  20.2 us
    reduce_scatter x1, waiting for transfers between devices, local(): lax.psum_scatter(lax.optimization_barrier(product.astype(jnp.bfloat16)).a...  13.5 us
    all_gather x1, waiting for transfers between devices, local(): lax.all_gather(lax.all_to_all(outgoing.reshape(expert_count, capacity, wi...  13.1 us
    dot_general x2, matrix products, one_block(): jnp.einsum('hqk,khv->qhv', weights.astype(jnp.bfloat16), value_rows, pref...  12.1 us
    dot_general x2, matrix products, one_block(): jnp.einsum('qhr,kr->hqk', query_rot, rot_block, preferred_element_type=jn...  11 us
  transfers between devices with their start and end apart: 4, of which 4 were waited for; matrix products, arithmetic and copies ran while one was open for 2% of the time, Pallas kernels for 0%

commit v1 on v0

--- a/solution.py
+++ b/solution.py
@@ -10,6 +10,17 @@
 EPSILON = 1e-06
 ROPE_BASE = 10000.0
 NEG_LARGE = -1e30
+
+
+def pass_along(block, mesh_axis, dim):
+    count = lax.axis_size(mesh_axis)
+    forward = [(i, (i + 1) % count) for i in range(count)]
+    parts = [block]
+    for hop in range(1, count):
+        parts = [lax.ppermute(parts[0], mesh_axis, forward), *parts]
+    whole = jnp.concatenate(parts, axis=dim)
+    shift = (lax.axis_index(mesh_axis) + 1) * parts[-1].shape[dim]
+    return jnp.roll(whole, shift, axis=dim)
 
 
 def rotary(values, positions):
@@ -72,7 +83,7 @@
         lax.all_gather(key_rot, "tp", axis=0, tiled=True),
     )
     lat_rows = lax.all_gather(paired[0], "sp", axis=0, tiled=True)
-    rot_rows = lax.all_gather(paired[1], "sp", axis=0, tiled=True)
+    rot_rows = pass_along(paired[1], "sp", 0)
     piece_rows = lat_rows.shape[0]
     key_block = piece_rows
     while key_block > 2048 and key_block % 2 == 0:

time: 298 us -> 368 us (1.23)
  starting transfers between devices: 7.08 us -> 52.6 us
  local copies, waits for them, and re-layouts: 17.9 us -> 37.9 us
  waiting for transfers between devices: 95.1 us -> 110 us
  blocking collectives: 97.9 us -> 86.8 us
    ppermute x0 -> x15, starting transfers between devices: none -> 45.5 us  [pass_along(): parts = [lax.ppermute(parts[0], mesh_axis, forward), *parts]]
    all_gather x1 -> x0, blocking collectives: 35.9 us -> none  [local(): rot_rows = lax.all_gather(paired[1], 'sp', axis=0, tiled=True)]
    ppermute x0 -> x15, waiting for transfers between devices: none -> 35.2 us  [pass_along(): parts = [lax.ppermute(parts[0], mesh_axis, forward), *parts]]
    all_to_all x1, blocking collectives: 52.8 us -> 77.7 us  [local(): lax.all_to_all(outgoing.reshape(expert_count, capacity, width), 'sp', spl...]
    all_gather x1, waiting for transfers between devices: 20.2 us -> 0.01 us  [local(): lat_rows = lax.all_gather(paired[0], 'sp', axis=0, tiled=True)]
    unnamed x14 -> x53, local copies, waits for them, and re-layouts: 1.96 us -> 21.1 us
  transfers between devices with their start and end apart: 4 -> 19, of which waited for: 4 -> 17; matrix products, arithmetic and copies ran while one was open for 2% -> 7% of each run, Pallas kernels for 0% -> 0%
where the time goes in v1:
time: 368 us; the launch traced here: 367 us
  waiting for transfers between devices  110 us (30%)
  blocking collectives  86.8 us (24%)
  starting transfers between devices  52.6 us (14%)
  matrix products  49.2 us (13%)
  local copies, waits for them, and re-layouts  37.9 us (10%)
  other arithmetic  16.8 us (5%)
  between operations  13.4 us (4%)
    all_to_all x1, blocking collectives, local(): lax.all_to_all(outgoing.reshape(expert_count, capacity, width), 'sp', spl...  77.7 us
    all_to_all x1, waiting for transfers between devices, local(): lax.all_to_all(summed, 'sp', split_axis=0, concat_axis=0, tiled=True)  48.2 us
    ppermute x15, starting transfers between devices, pass_along(): parts = [lax.ppermute(parts[0], mesh_axis, forward), *parts]  45.5 us
    ppermute x15, waiting for transfers between devices, pass_along(): parts = [lax.ppermute(parts[0], mesh_axis, forward), *parts]  35.2 us
    unnamed x53, local copies, waits for them, and re-layouts  21.1 us
    reduce_scatter x1, waiting for transfers between devices, local(): lax.psum_scatter(lax.optimization_barrier(product.astype(jnp.bfloat16)).a...  13.5 us
    all_gather x1, waiting for transfers between devices, local(): lax.all_gather(lax.all_to_all(outgoing.reshape(expert_count, capacity, wi...  13 us
    dot_general x2, matrix products, one_block(): jnp.einsum('hqk,khv->qhv', weights.astype(jnp.bfloat16), value_rows, pref...  12.1 us
  transfers between devices with their start and end apart: 19, of which 17 were waited for; matrix products, arithmetic and copies ran while one was open for 7% of the time, Pallas kernels for 0%

profile of v1, /device:TPU:12, one launch (start us, length us, event | category | flops | bytes accessed | tf_op | source)
XLA Modules:
  0.0 366.9 jit_solution(14718583798354669532)
XLA Ops:
  7.6 1.9 all_gather.14
  9.5 1.5 collective-permute-start
  11.0 3.3 collective-permute-done
  14.9 4.2 %collective-permute-done.1 = bf16[256,64]{0,1:T(8,128)(2,1)S(1)} collective-permute-done((bf16[256,64]{0,1:T(8,128)(2,1)S(1)}, bf16[256,64]{0,1:T(8,128)(2,1)S(1)}, u32[]{:S(2)}, u32[]{:S(2)}) %collective-permute-start.1) | collective-permute-done | bytes 32800 | tf_op jit(solution)/shard_map/ppermute | solution.py:20
  19.8 4.1 %collective-permute-done.2 = bf16[256,64]{0,1:T(8,128)(2,1)S(1)} collective-permute-done((bf16[256,64]{0,1:T(8,128)(2,1)S(1)}, bf16[256,64]{0,1:T(8,128)(2,1)S(1)}, u32[]{:S(2)}, u32[]{:S(2)}) %collective-permute-start.2) | collective-permute-done | bytes 32800 | tf_op jit(solution)/shard_map/ppermute | solution.py:20
  23.9 1.6 collective-permute-start.3
  25.5 3.3 all_gather.12
  28.9 4.2 %collective-permute-start.4 = (bf16[256,64]{0,1:T(8,128)(2,1)S(1)}, bf16[256,64]{0,1:T(8,128)(2,1)S(1)}, u32[]{:S(2)}, u32[]{:S(2)}) collective-permute-start(bf16[256,64]{0,1:T(8,128)(2,1)S(1)} %collective-permute-done.3), channel_id=1, source_target_pairs={{0,2},{2,4},{4,6},{6,8},{8,10},{10,12},{12,14},{14,16},{16,18},{18... | collective-permute-start | bytes 98312 | tf_op jit(solution)/shard_map/ppermute | solution.py:20
  33.1 1.6 collective-permute-done.4
  34.7 2.3 collective-permute-start.5
  39.5 3.1 collective-permute-start.6
  44.4 4.7 %collective-permute-start.7 = (bf16[256,64]{0,1:T(8,128)(2,1)S(1)}, bf16[256,64]{0,1:T(8,128)(2,1)S(1)}, u32[]{:S(2)}, u32[]{:S(2)}) collective-permute-start(bf16[256,64]{0,1:T(8,128)(2,1)S(1)} %collective-permute-done.6), channel_id=1, source_target_pairs={{0,2},{2,4},{4,6},{6,8},{8,10},{10,12},{12,14},{14,16},{16,18},{18... | collective-permute-start | bytes 98312 | tf_op jit(solution)/shard_map/ppermute | solution.py:20
  49.2 1.6 collective-permute-done.7
  50.8 4.3 %collective-permute-start.8 = (bf16[256,64]{0,1:T(8,128)(2,1)S(1)}, bf16[256,64]{0,1:T(8,128)(2,1)S(1)}, u32[]{:S(2)}, u32[]{:S(2)}) collective-permute-start(bf16[256,64]{0,1:T(8,128)(2,1)S(1)} %collective-permute-done.7), channel_id=1, source_target_pairs={{0,2},{2,4},{4,6},{6,8},{8,10},{10,12},{12,14},{14,16},{16,18},{18... | collective-permute-start | bytes 98312 | tf_op jit(solution)/shard_map/ppermute | solution.py:20
  56.6 4.1 %collective-permute-start.9 = (bf16[256,64]{0,1:T(8,128)(2,1)S(1)}, bf16[256,64]{0,1:T(8,128)(2,1)S(1)}, u32[]{:S(2)}, u32[]{:S(2)}) collective-permute-start(bf16[256,64]{0,1:T(8,128)(2,1)S(1)} %collective-permute-done.8), channel_id=1, source_target_pairs={{0,2},{2,4},{4,6},{6,8},{8,10},{10,12},{12,14},{14,16},{16,18},{18... | collective-permute-start | bytes 98312 | tf_op jit(solution)/shard_map/ppermute | solution.py:20
  62.4 4.1 %collective-permute-start.10 = (bf16[256,64]{0,1:T(8,128)(2,1)S(1)}, bf16[256,64]{0,1:T(8,128)(2,1)S(1)}, u32[]{:S(2)}, u32[]{:S(2)}) collective-permute-start(bf16[256,64]{0,1:T(8,128)(2,1)S(1)} %collective-permute-done.9), channel_id=1, source_target_pairs={{0,2},{2,4},{4,6},{6,8},{8,10},{10,12},{12,14},{14,16},{16,18},{18... | collective-permute-start | bytes 98312 | tf_op jit(solution)/shard_map/ppermute | solution.py:20
  66.6 1.8 collective-permute-done.10
  68.4 4.0 %collective-permute-start.11 = (bf16[256,64]{0,1:T(8,128)(2,1)S(1)}, bf16[256,64]{0,1:T(8,128)(2,1)S(1)}, u32[]{:S(2)}, u32[]{:S(2)}) collective-permute-start(bf16[256,64]{0,1:T(8,128)(2,1)S(1)} %collective-permute-done.10), channel_id=1, source_target_pairs={{0,2},{2,4},{4,6},{6,8},{8,10},{10,12},{12,14},{14,16},{16,18},{18... | collective-permute-start | bytes 98312 | tf_op jit(solution)/shard_map/ppermute | solution.py:20
  74.0 4.6 %collective-permute-start.12 = (bf16[256,64]{0,1:T(8,128)(2,1)S(1)}, bf16[256,64]{0,1:T(8,128)(2,1)S(1)}, u32[]{:S(2)}, u32[]{:S(2)}) collective-permute-start(bf16[256,64]{0,1:T(8,128)(2,1)S(1)} %collective-permute-done.11), channel_id=1, source_target_pairs={{0,2},{2,4},{4,6},{6,8},{8,10},{10,12},{12,14},{14,16},{16,18},{18... | collective-permute-start | bytes 98312 | tf_op jit(solution)/shard_map/ppermute | solution.py:20
  78.5 2.9 collective-permute-done.12
  81.4 4.3 %collective-permute-start.13 = (bf16[256,64]{0,1:T(8,128)(2,1)S(1)}, bf16[256,64]{0,1:T(8,128)(2,1)S(1)}, u32[]{:S(2)}, u32[]{:S(2)}) collective-permute-start(bf16[256,64]{0,1:T(8,128)(2,1)S(1)} %collective-permute-done.12), channel_id=1, source_target_pairs={{0,2},{2,4},{4,6},{6,8},{8,10},{10,12},{12,14},{14,16},{16,18},{18... | collective-permute-start | bytes 98312 | tf_op jit(solution)/shard_map/ppermute | solution.py:20
  85.7 4.6 %collective-permute-done.13 = bf16[256,64]{0,1:T(8,128)(2,1)S(1)} collective-permute-done((bf16[256,64]{0,1:T(8,128)(2,1)S(1)}, bf16[256,64]{0,1:T(8,128)(2,1)S(1)}, u32[]{:S(2)}, u32[]{:S(2)}) %collective-permute-start.13) | collective-permute-done | bytes 32800 | tf_op jit(solution)/shard_map/ppermute | solution.py:20
  91.8 6.0 %collective-permute-done.14 = bf16[256,64]{0,1:T(8,128)(2,1)S(1)} collective-permute-done((bf16[256,64]{0,1:T(8,128)(2,1)S(1)}, bf16[256,64]{0,1:T(8,128)(2,1)S(1)}, u32[]{:S(2)}, u32[]{:S(2)}) %collective-permute-start.14) | collective-permute-done | bytes 32800 | tf_op jit(solution)/shard_map/ppermute | solution.py:20
  117.6 44.2 %conditional.1 = (f32[4,256]{1,0:T(4,128)}, f32[256,4,128]{0,2,1:T(8,128)}) conditional(s32[]{:T(128)} %convert_element_type.80, () %tuple.45, (bf16[4096,256]{1,0:T(8,128)(2,1)}, s32[]{:T(128)}, s32[]{:T(128)}, bf16[8192,64]{0,1:T(8,128)(2,1)}, bf16[256,512]{1,0:T(8,128)(2,1)S(1)}, /*index=5*/s32[256]{0:T(256)S(1)}, s32[256]{0:T(256)S(1)}, ...), branch_computations={%region_0.1_spmd, %region_1.6_spmd.clone} | conditional | flops 2439948032 | bytes 85153400 | solution.py:141
  119.3 42.5 %while.26 = (s32[]{:T(128)}, f32[4,256]{1,0:T(4,128)S(1)}, f32[4,256]{1,0:T(4,128)}, f32[256,4,128]{0,2,1:T(8,128)}, s32[2]{0:T(128)S(1)}, /*index=5*/s32[256]{0...) while((s32[]{:T(128)}, f32[4,256]{1,0:T(4,128)S(1)}, ...), condition=%wide.region_5.5_spmd.clone, body=%wide.region_2.4_spmd.clone.sunk | while | flops 2439944192 | bytes 82004296 | solution.py:127
  119.4 2.0 convolution_convert_fusion.5
  124.4 5.5 %fusion.96 = (f32[4,256]{1,0:T(4,128)S(1)}, f32[4,256,2048]{1,2,0:T(8,128)}) fusion(bf16[256,4,64]{0,2,1:T(8,128)(2,1)S(1)} %get-tuple-element.690, bf16[2,2048,64]{1,2,0:T(8,128)(2,1)S(1)} %get-tuple-element.689, s32[]{:T(128)} %get-tuple-element.666, f32[4,2048,256]{2,1,0:T(8,128)S(1)} %fusion.95, pred[256,2048]{0,1:T(8,128)(4,1)S(1)} %broadcast_compare_fusion.2), kind=kOutput, calls=%fused_computation.138.clone.1 | convolution fusion | flops 276823040 | bytes 17698820 | tf_op jit(solution)/shard_map/cond/branch_1_fun/while/body/eval_jaxpr/qhr,kr->hqk/dot_general | solution.py:108
  129.9 2.1 convolution_convert_fusion.6
  132.1 6.0 %fusion.100 = f32[256,4,128]{0,2,1:T(8,128)} fusion(bf16[2048,4,128]{0,2,1:T(8,128)(2,1)S(1)} %bitcast.115, f32[4,256,2048]{1,2,0:T(8,128)} %get-tuple-element.650, f32[4,256]{1,0:T(4,128)S(1)} %get-tuple-element.681, pred[256,2048]{0,1:T(8,128)(4,1)S(1)} %broadcast_compare_fusion.2, f32[256,4,128]{0,2,1:T(8,128)} %get-tuple-element.669, ...), kind=kOutput, calls=%fused_computation.15.clone.1 | convolution fusion | flops 543555584 | bytes 12066817 | tf_op jit(solution)/shard_map/cond/branch_1_fun/while/body/eval_jaxpr/hqk,khv->qhv/dot_general | solution.py:118
  138.1 1.5 fusion.98
  140.2 2.0 convolution_convert_fusion.5
  145.3 5.5 %fusion.96 = (f32[4,256]{1,0:T(4,128)S(1)}, f32[4,256,2048]{1,2,0:T(8,128)}) fusion(bf16[256,4,64]{0,2,1:T(8,128)(2,1)S(1)} %get-tuple-element.690, bf16[2,2048,64]{1,2,0:T(8,128)(2,1)S(1)} %get-tuple-element.689, s32[]{:T(128)} %get-tuple-element.666, f32[4,2048,256]{2,1,0:T(8,128)S(1)} %fusion.95, pred[256,2048]{0,1:T(8,128)(4,1)S(1)} %broadcast_compare_fusion.2), kind=kOutput, calls=%fused_computation.138.clone.1 | convolution fusion | flops 276823040 | bytes 17698820 | tf_op jit(solution)/shard_map/cond/branch_1_fun/while/body/eval_jaxpr/qhr,kr->hqk/dot_general | solution.py:108
  150.8 2.1 convolution_convert_fusion.6
  153.0 6.1 %fusion.100 = f32[256,4,128]{0,2,1:T(8,128)} fusion(bf16[2048,4,128]{0,2,1:T(8,128)(2,1)S(1)} %bitcast.115, f32[4,256,2048]{1,2,0:T(8,128)} %get-tuple-element.650, f32[4,256]{1,0:T(4,128)S(1)} %get-tuple-element.681, pred[256,2048]{0,1:T(8,128)(4,1)S(1)} %broadcast_compare_fusion.2, f32[256,4,128]{0,2,1:T(8,128)} %get-tuple-element.669, ...), kind=kOutput, calls=%fused_computation.15.clone.1 | convolution fusion | flops 543555584 | bytes 12066817 | tf_op jit(solution)/shard_map/cond/branch_1_fun/while/body/eval_jaxpr/hqk,khv->qhv/dot_general | solution.py:118
  159.0 1.5 fusion.98
  163.2 3.9 %all_to_all.29 = bf16[2,128,512]{2,1,0:T(8,128)(2,1)S(1)} all-to-all(bf16[2,128,512]{2,1,0:T(8,128)(2,1)S(1)} %copy.65), channel_id=1, replica_groups=mesh['sp'=16,'tp'=2] {'tp'}, dimensions={0} | all-to-all | bytes 524288 | tf_op jit(solution)/shard_map/all_to_all | solution.py:149
  167.3 3.0 multiply_reduce_fusion.1
  173.4 3.5 scatter_custom_fusion
  176.9 77.7 %all_to_all.30 = bf16[16,32,2048]{2,1,0:T(8,128)(2,1)} all-to-all(bf16[16,32,2048]{2,1,0:T(8,128)(2,1)S(1)} %bitcast.116), channel_id=1, replica_groups=mesh['sp'=16,'tp'=2] {'sp'}, dimensions={0} | all-to-all | bytes 4194304 | tf_op jit(solution)/shard_map/all_to_all | solution.py:177
  254.6 13.0 %all-gather.5.cloned.1.call-done = bf16[32,32,2048]{2,1,0:T(8,128)(2,1)} async-done(((bf16[16,32,2048]{2,1,0:T(8,128)(2,1)}), bf16[32,32,2048]{2,1,0:T(8,128)(2,1)}) %all-gather.5.cloned.1.call-update) | async-done | bytes 4194320 | tf_op jit(solution)/shard_map/all_gather | solution.py:176
  267.7 3.7 %fusion.36 = f32[32,32,256]{2,1,0:T(8,128)S(1)} fusion(bf16[32,32,2048]{2,1,0:T(8,128)(2,1)} %all-gather.5.cloned.1.call-done, bf16[1,2048,256]{2,1,0:T(8,128)(2,1)} %param.29), kind=kOutput, calls=%fused_computation.58 | convolution fusion | flops 1073741824 | bytes 6291456 | tf_op jit(solution)/shard_map/dot_general | solution.py:188
  271.4 8.5 %convolution_convert_fusion.2 = bf16[32,32,2048]{2,1,0:T(8,128)(2,1)} fusion(bf16[32,32,2048]{2,1,0:T(8,128)(2,1)} %all-gather.5.cloned.1.call-done, bf16[1,256,2048]{2,1,0:T(8,128)(2,1)S(1)} %copy-done, bf16[1,2048,256]{2,1,0:T(8,128)(2,1)S(1)} %copy-done.9, f32[32,32,256]{2,1,0:T(8,128)S(1)} %fusion.36), kind=kOutput, calls=%fused_computation.49 | convolution fusion | flops 2151153664 | bytes 11534336 | tf_op jit(solution)/shard_map/dot_general | solution.py:191
  280.0 13.5 %reduce-scatter.2.cloned.1.call-done = bf16[16,32,2048]{2,1,0:T(8,128)(2,1)} async-done(((bf16[32,32,2048]{2,1,0:T(8,128)(2,1)}), bf16[16,32,2048]{2,1,0:T(8,128)(2,1)}) %reduce-scatter.2.cloned.1.call-update) | async-done | bytes 2097168 | tf_op jit(solution)/shard_map/reduce_scatter | solution.py:192
  293.5 7.0 %all-to-all-start.2 = ((bf16[16,32,2048]{2,1,0:T(8,128)(2,1)}), bf16[16,32,2048]{2,1,0:T(8,128)(2,1)S(1)}, u32[]{:S(2)}, u32[]{:S(2)}) async-start(bf16[16,32,2048]{2,1,0:T(8,128)(2,1)} %reduce-scatter.2.cloned.1.call-done), calls=%async_computation.3 | async-start | bytes 4194304 | tf_op jit(solution)/shard_map/all_to_all | solution.py:200
  300.6 48.2 %all-to-all-done.2 = bf16[16,32,2048]{2,1,0:T(8,128)(2,1)S(1)} async-done(((bf16[16,32,2048]{2,1,0:T(8,128)(2,1)}), bf16[16,32,2048]{2,1,0:T(8,128)(2,1)S(1)}, u32[]{:S(2)}, u32[]{:S(2)}) %all-to-all-start.2) | async-done | bytes 2097184 | tf_op jit(solution)/shard_map/all_to_all | solution.py:200
  348.8 2.3 gather_fusion
  351.2 3.4 reshape.238
  354.6 4.8 %multiply_reduce_fusion = f32[128,2048]{1,0:T(8,128)S(1)} fusion(f32[128,2,2048]{2,1,0:T(2,128)} %reshape.238, f32[128,2]{1,0:T(8,128)S(1)} %copy.62), kind=kLoop, calls=%fused_computation.53 | loop fusion | flops 786432 | bytes 3146752 | tf_op jit(solution)/shard_map/reduce_sum | solution.py:202
  (145 shorter events, 48.0 us)
Async XLA Ops:
  6.5 264.9 %copy-start = (bf16[1,256,2048]{2,1,0:T(8,128)(2,1)S(1)}, bf16[1,256,2048]{2,1,0:T(8,128)(2,1)}, u32[]{:S(2)}) copy-start(bf16[1,256,2048]{2,1,0:T(8,128)(2,1)} %param.31) | copy-start | bytes 3145732
  6.5 111.0 %copy-start.6 = (bf16[256,512]{1,0:T(8,128)(2,1)S(1)}, bf16[256,512]{1,0:T(8,128)(2,1)}, u32[]{:S(2)}) copy-start(bf16[256,512]{1,0:T(8,128)(2,1)} %param.19) | copy-start | bytes 786436
  6.5 111.0 %copy-start.3 = (bf16[256,512]{1,0:T(8,128)(2,1)S(1)}, bf16[256,512]{1,0:T(8,128)(2,1)}, u32[]{:S(2)}) copy-start(bf16[256,512]{1,0:T(8,128)(2,1)} %param.23) | copy-start | bytes 786436
  6.5 111.0 %copy-start.4 = (bf16[256,512]{1,0:T(8,128)(2,1)S(1)}, bf16[256,512]{1,0:T(8,128)(2,1)}, u32[]{:S(2)}) copy-start(bf16[256,512]{1,0:T(8,128)(2,1)} %param.24) | copy-start | bytes 786436
  6.5 111.0 %all-gather.3.cloned.1.call-start = ((), (), s32[]{:S(2)}) async-start(), calls=%async_computation.4 | async-start | bytes 2228224 | tf_op jit(solution)/shard_map/all_gather | solution.py:85
  9.5 4.8 %collective-permute-start = (bf16[256,64]{0,1:T(8,128)(2,1)S(1)}, bf16[256,64]{0,1:T(8,128)(2,1)S(1)}, u32[]{:S(2)}, u32[]{:S(2)}) collective-permute-start(bf16[256,64]{0,1:T(8,128)(2,1)S(1)} %all_gather.14), channel_id=1, source_target_pairs={{0,2},{2,4},{4,6},{6,8},{8,10},{10,12},{12,14},{14,16},{16,18},{18... | collective-permute-start | bytes 98312 | tf_op jit(solution)/shard_map/ppermute | solution.py:20
  14.3 4.8 %collective-permute-start.1 = (bf16[256,64]{0,1:T(8,128)(2,1)S(1)}, bf16[256,64]{0,1:T(8,128)(2,1)S(1)}, u32[]{:S(2)}, u32[]{:S(2)}) collective-permute-start(bf16[256,64]{0,1:T(8,128)(2,1)S(1)} %collective-permute-done), channel_id=1, source_target_pairs={{0,2},{2,4},{4,6},{6,8},{8,10},{10,12},{12,14},{14,16},{16,18},{18... | collective-permute-start | bytes 98312 | tf_op jit(solution)/shard_map/ppermute | solution.py:20
  19.1 4.8 %collective-permute-start.2 = (bf16[256,64]{0,1:T(8,128)(2,1)S(1)}, bf16[256,64]{0,1:T(8,128)(2,1)S(1)}, u32[]{:S(2)}, u32[]{:S(2)}) collective-permute-start(bf16[256,64]{0,1:T(8,128)(2,1)S(1)} %collective-permute-done.1), channel_id=1, source_target_pairs={{0,2},{2,4},{4,6},{6,8},{8,10},{10,12},{12,14},{14,16},{16,18},{18... | collective-permute-start | bytes 98312 | tf_op jit(solution)/shard_map/ppermute | solution.py:20
  23.9 5.0 %collective-permute-start.3 = (bf16[256,64]{0,1:T(8,128)(2,1)S(1)}, bf16[256,64]{0,1:T(8,128)(2,1)S(1)}, u32[]{:S(2)}, u32[]{:S(2)}) collective-permute-start(bf16[256,64]{0,1:T(8,128)(2,1)S(1)} %collective-permute-done.2), channel_id=1, source_target_pairs={{0,2},{2,4},{4,6},{6,8},{8,10},{10,12},{12,14},{14,16},{16,18},{18... | collective-permute-start | bytes 98312 | tf_op jit(solution)/shard_map/ppermute | solution.py:20
  28.9 238.8 %all-gather.5.cloned.1.call-start = ((), (), s32[]{:S(2)}) async-start(), calls=%async_computation.5 | async-start | bytes 6291456 | tf_op jit(solution)/shard_map/all_gather | solution.py:176
  28.9 5.8 %collective-permute-start.4 = (bf16[256,64]{0,1:T(8,128)(2,1)S(1)}, bf16[256,64]{0,1:T(8,128)(2,1)S(1)}, u32[]{:S(2)}, u32[]{:S(2)}) collective-permute-start(bf16[256,64]{0,1:T(8,128)(2,1)S(1)} %collective-permute-done.3), channel_id=1, source_target_pairs={{0,2},{2,4},{4,6},{6,8},{8,10},{10,12},{12,14},{14,16},{16,18},{18... | collective-permute-start | bytes 98312 | tf_op jit(solution)/shard_map/ppermute | solution.py:20
  34.7 4.8 %collective-permute-start.5 = (bf16[256,64]{0,1:T(8,128)(2,1)S(1)}, bf16[256,64]{0,1:T(8,128)(2,1)S(1)}, u32[]{:S(2)}, u32[]{:S(2)}) collective-permute-start(bf16[256,64]{0,1:T(8,128)(2,1)S(1)} %collective-permute-done.4), channel_id=1, source_target_pairs={{0,2},{2,4},{4,6},{6,8},{8,10},{10,12},{12,14},{14,16},{16,18},{18... | collective-permute-start | bytes 98312 | tf_op jit(solution)/shard_map/ppermute | solution.py:20
  39.5 4.9 %collective-permute-start.6 = (bf16[256,64]{0,1:T(8,128)(2,1)S(1)}, bf16[256,64]{0,1:T(8,128)(2,1)S(1)}, u32[]{:S(2)}, u32[]{:S(2)}) collective-permute-start(bf16[256,64]{0,1:T(8,128)(2,1)S(1)} %collective-permute-done.5), channel_id=1, source_target_pairs={{0,2},{2,4},{4,6},{6,8},{8,10},{10,12},{12,14},{14,16},{16,18},{18... | collective-permute-start | bytes 98312 | tf_op jit(solution)/shard_map/ppermute | solution.py:20
  44.4 6.3 %collective-permute-start.7 = (bf16[256,64]{0,1:T(8,128)(2,1)S(1)}, bf16[256,64]{0,1:T(8,128)(2,1)S(1)}, u32[]{:S(2)}, u32[]{:S(2)}) collective-permute-start(bf16[256,64]{0,1:T(8,128)(2,1)S(1)} %collective-permute-done.6), channel_id=1, source_target_pairs={{0,2},{2,4},{4,6},{6,8},{8,10},{10,12},{12,14},{14,16},{16,18},{18... | collective-permute-start | bytes 98312 | tf_op jit(solution)/shard_map/ppermute | solution.py:20
  50.8 5.9 %collective-permute-start.8 = (bf16[256,64]{0,1:T(8,128)(2,1)S(1)}, bf16[256,64]{0,1:T(8,128)(2,1)S(1)}, u32[]{:S(2)}, u32[]{:S(2)}) collective-permute-start(bf16[256,64]{0,1:T(8,128)(2,1)S(1)} %collective-permute-done.7), channel_id=1, source_target_pairs={{0,2},{2,4},{4,6},{6,8},{8,10},{10,12},{12,14},{14,16},{16,18},{18... | collective-permute-start | bytes 98312 | tf_op jit(solution)/shard_map/ppermute | solution.py:20
  56.6 5.7 %collective-permute-start.9 = (bf16[256,64]{0,1:T(8,128)(2,1)S(1)}, bf16[256,64]{0,1:T(8,128)(2,1)S(1)}, u32[]{:S(2)}, u32[]{:S(2)}) collective-permute-start(bf16[256,64]{0,1:T(8,128)(2,1)S(1)} %collective-permute-done.8), channel_id=1, source_target_pairs={{0,2},{2,4},{4,6},{6,8},{8,10},{10,12},{12,14},{14,16},{16,18},{18... | collective-permute-start | bytes 98312 | tf_op jit(solution)/shard_map/ppermute | solution.py:20
  62.4 6.0 %collective-permute-start.10 = (bf16[256,64]{0,1:T(8,128)(2,1)S(1)}, bf16[256,64]{0,1:T(8,128)(2,1)S(1)}, u32[]{:S(2)}, u32[]{:S(2)}) collective-permute-start(bf16[256,64]{0,1:T(8,128)(2,1)S(1)} %collective-permute-done.9), channel_id=1, source_target_pairs={{0,2},{2,4},{4,6},{6,8},{8,10},{10,12},{12,14},{14,16},{16,18},{18... | collective-permute-start | bytes 98312 | tf_op jit(solution)/shard_map/ppermute | solution.py:20
  68.4 5.6 %collective-permute-start.11 = (bf16[256,64]{0,1:T(8,128)(2,1)S(1)}, bf16[256,64]{0,1:T(8,128)(2,1)S(1)}, u32[]{:S(2)}, u32[]{:S(2)}) collective-permute-start(bf16[256,64]{0,1:T(8,128)(2,1)S(1)} %collective-permute-done.10), channel_id=1, source_target_pairs={{0,2},{2,4},{4,6},{6,8},{8,10},{10,12},{12,14},{14,16},{16,18},{18... | collective-permute-start | bytes 98312 | tf_op jit(solution)/shard_map/ppermute | solution.py:20
  74.0 7.4 %collective-permute-start.12 = (bf16[256,64]{0,1:T(8,128)(2,1)S(1)}, bf16[256,64]{0,1:T(8,128)(2,1)S(1)}, u32[]{:S(2)}, u32[]{:S(2)}) collective-permute-start(bf16[256,64]{0,1:T(8,128)(2,1)S(1)} %collective-permute-done.11), channel_id=1, source_target_pairs={{0,2},{2,4},{4,6},{6,8},{8,10},{10,12},{12,14},{14,16},{16,18},{18... | collective-permute-start | bytes 98312 | tf_op jit(solution)/shard_map/ppermute | solution.py:20
  81.4 8.9 %collective-permute-start.13 = (bf16[256,64]{0,1:T(8,128)(2,1)S(1)}, bf16[256,64]{0,1:T(8,128)(2,1)S(1)}, u32[]{:S(2)}, u32[]{:S(2)}) collective-permute-start(bf16[256,64]{0,1:T(8,128)(2,1)S(1)} %collective-permute-done.12), channel_id=1, source_target_pairs={{0,2},{2,4},{4,6},{6,8},{8,10},{10,12},{12,14},{14,16},{16,18},{18... | collective-permute-start | bytes 98312 | tf_op jit(solution)/shard_map/ppermute | solution.py:20
  90.3 7.5 %collective-permute-start.14 = (bf16[256,64]{0,1:T(8,128)(2,1)S(1)}, bf16[256,64]{0,1:T(8,128)(2,1)S(1)}, u32[]{:S(2)}, u32[]{:S(2)}) collective-permute-start(bf16[256,64]{0,1:T(8,128)(2,1)S(1)} %collective-permute-done.13), channel_id=1, source_target_pairs={{0,2},{2,4},{4,6},{6,8},{8,10},{10,12},{12,14},{14,16},{16,18},{18... | collective-permute-start | bytes 98312 | tf_op jit(solution)/shard_map/ppermute | solution.py:20
  117.6 49.7 %copy-start.5 = (bf16[128,2048]{1,0:T(8,128)(2,1)S(1)}, bf16[128,2048]{1,0:T(8,128)(2,1)}, u32[]{:S(2)}) copy-start(bf16[128,2048]{1,0:T(8,128)(2,1)} %param.18) | copy-start | bytes 1572868
  119.4 3.3 copy-start.10
  129.9 8.2 %slice-start = ((s8[8388608]{0:T(1024)(128)(4,1)}), s8[4194304]{0:T(1024)(128)(4,1)S(1)}, s32[]{:S(2)}) async-start(s8[8388608]{0:T(1024)(128)(4,1)} %bitcast.110), calls=%async_computation.7 | async-start | bytes 8388608 | tf_op jit(solution)/shard_map/cond/branch_1_fun/while
  132.1 6.0 %slice-start.1 = ((s8[8388608]{0:T(1024)(128)(4,1)}), s8[4194304]{0:T(1024)(128)(4,1)S(1)}, s32[]{:S(2)}) async-start(s8[8388608]{0:T(1024)(128)(4,1)} %bitcast.110), calls=%async_computation.8 | async-start | bytes 8388608 | tf_op jit(solution)/shard_map/cond/branch_1_fun/while
  138.1 2.1 copy-start.11
  140.2 3.3 copy-start.10
  150.8 8.2 %slice-start = ((s8[8388608]{0:T(1024)(128)(4,1)}), s8[4194304]{0:T(1024)(128)(4,1)S(1)}, s32[]{:S(2)}) async-start(s8[8388608]{0:T(1024)(128)(4,1)} %bitcast.110), calls=%async_computation.7 | async-start | bytes 8388608 | tf_op jit(solution)/shard_map/cond/branch_1_fun/while
  152.9 6.1 %slice-start.1 = ((s8[8388608]{0:T(1024)(128)(4,1)}), s8[4194304]{0:T(1024)(128)(4,1)S(1)}, s32[]{:S(2)}) async-start(s8[8388608]{0:T(1024)(128)(4,1)} %bitcast.110), calls=%async_computation.8 | async-start | bytes 8388608 | tf_op jit(solution)/shard_map/cond/branch_1_fun/while
  159.0 2.8 copy-start.11
  162.9 8.5 %copy-start.7 = (f32[2048]{0:T(1024)S(1)}, f32[2048]{0:T(1024)}, u32[]{:S(2)}) copy-start(f32[2048]{0:T(1024)} %param.26) | copy-start | bytes 24580
  170.3 1.1 copy-start.1
  254.6 16.9 %copy-start.9 = (bf16[1,2048,256]{2,1,0:T(8,128)(2,1)S(1)}, bf16[1,2048,256]{2,1,0:T(8,128)(2,1)}, u32[]{:S(2)}) copy-start(bf16[1,2048,256]{2,1,0:T(8,128)(2,1)} %param.30) | copy-start | bytes 3145732
  254.6 38.9 %reduce-scatter.2.cloned.1.call-start = ((), (), s32[]{:S(2)}) async-start(), calls=%async_computation.6 | async-start | bytes 6291456 | tf_op jit(solution)/shard_map/reduce_scatter | solution.py:192
  280.0 20.5 %copy-start.8 = (f32[128,2]{0,1:T(2,128)S(1)}, f32[128,2]{0,1:T(2,128)}, u32[]{:S(2)}) copy-start(f32[128,2]{0,1:T(2,128)} %param.28) | copy-start | bytes 3076
  293.5 55.4 %all-to-all-start.2 = ((bf16[16,32,2048]{2,1,0:T(8,128)(2,1)}), bf16[16,32,2048]{2,1,0:T(8,128)(2,1)S(1)}, u32[]{:S(2)}, u32[]{:S(2)}) async-start(bf16[16,32,2048]{2,1,0:T(8,128)(2,1)} %reduce-scatter.2.cloned.1.call-done), calls=%async_computation.3 | async-start | bytes 4194304 | tf_op jit(solution)/shard_map/all_to_all | solution.py:200
  351.2 8.2 %copy-start.2 = (f32[128,2048]{1,0:T(8,128)S(1)}, f32[128,2048]{1,0:T(8,128)}, u32[]{:S(2)}) copy-start(f32[128,2048]{1,0:T(8,128)} %copy-done.1) | copy-start | bytes 3145732
Sparse Core Ops, SparseCore 0:
  29.0 69.5 all-gather.2
  254.7 12.9 all-gather.4
  280.1 13.2 reduce-scatter.1
